TPU v7x, 512 devices: a whole 4x8x8 slice. The times are simulated.
512 devices in a mesh: kv: 32 (over z, x), tp: 16 (over y, core).
Axes of the slice: x: 4, y: 8, z: 8, core: 2. Of those that a mesh axis runs over, the one named last changes fastest.
Arguments:
- tokens: bfloat16 [16, 4096], P(None, ('kv', 'tp')), may hold values from -24 to 24
- live_lengths: int32 [16], replicated, may hold values from 256 to 16384, as said below
- kv_cache: bfloat16 [16, 16384, 2048], P(None, 'kv', 'tp'), may hold values from -128 to 128
- gate_sums: float32 [16, 16, 16384], P(None, 'tp', 'kv'), may hold values from -16384 to 0, as said below
- w_query: bfloat16 [4096, 4096], P('kv', 'tp'), may hold values from -0.09375 to 0.09375
- w_key: bfloat16 [4096, 1024], P('kv', 'tp'), may hold values from -0.09375 to 0.09375
- w_value: bfloat16 [4096, 1024], P('kv', 'tp'), may hold values from -0.09375 to 0.09375
- w_forget: bfloat16 [4096, 16], replicated, may hold values from -0.09375 to 0.09375
- forget_bias: float32 [16], replicated, may hold values from -1 to 2
- w_out: bfloat16 [4096, 4096], P('tp', 'kv'), may hold values from -0.75 to 0.75
- first_gain: float32 [4096], P(('kv', 'tp')), may hold values from 0 to 4
- w_gate: bfloat16 [4096, 11264], P('kv', 'tp'), may hold values from -0.09375 to 0.09375
- w_up: bfloat16 [4096, 11264], P('kv', 'tp'), may hold values from -0.09375 to 0.09375
- w_down: bfloat16 [11264, 4096], P('tp', 'kv'), may hold values from -0.109375 to 0.109375
- second_gain: float32 [4096], P(('kv', 'tp')), may hold values from 0 to 4
Outputs:
- layer_out: bfloat16 [16, 4096], P(None, ('kv', 'tp'))
Inputs may be any that keep to these rules, and one draw needn't show every extreme that they name: `live_lengths`: at least one sequence has length exactly 16384. `gate_sums`: entries at positions at or beyond the sequence's length are 0.
All inputs are finite; a program needn't handle non-finite values.
Results may differ from a plain program's by a relative error of at most 0.019.
Values may be sent and summed in bfloat16 or wider, within the bound.
A program may use at most 64 MiB of HBM per device.

v0:
```python
import jax
import jax.numpy as jnp
from jax import lax
from jax.sharding import Mesh
from jax.sharding import PartitionSpec as P

D = 4096
DH = 64
GROUP = 4
KV = ("kv_0", "kv_1")
KV_TP = ("kv_0", "kv_1", "tp")


EPSILON = 1e-05
EMPTY_SCORE = -1e30


def sent_to_all(shard, axis):
    devices = lax.axis_size(axis)
    return lax.all_to_all(
        jnp.broadcast_to(shard[None], (devices, *shard.shape)), axis, 0, 0, tiled=True
    )


def over_copies(shard, axis):
    everything = sent_to_all(shard, axis)
    return jnp.sum(everything, axis=0)


def packed_total(arrays, axis):
    ends = [0]
    for a in arrays:
        ends.append(ends[-1] + a.size)
    running = over_copies(jnp.concatenate([a.ravel() for a in arrays]), axis)
    return tuple((running[b:e].reshape(a.shape) for a, b, e in zip(arrays, ends, ends[1:])))


def gather_turned(arrays, axis, dims):
    turned = [jnp.moveaxis(a, dim, 0) for a, dim in zip(arrays, dims)]
    widths = [t[0].size for t in turned]
    both = jnp.concatenate([t.reshape(-1, w) for t, w in zip(turned, widths)], axis=1)
    result = lax.all_gather(both, axis, axis=0, tiled=True)
    tiles = jnp.split(result, [sum(widths[:k]) for k in range(1, len(widths))], axis=1)
    return tuple(
        (
            jnp.moveaxis(b.reshape(-1, *t.shape[1:]), 0, dim)
            for b, t, dim in zip(tiles, turned, dims)
        )
    )


def collected_together(shard, axis):
    leaves = jax.tree.leaves(shard)
    turns = sorted(range(len(leaves)), key=lambda k: -leaves[k].size)
    width = (1, *leaves[turns[0]].shape)[-1]
    lines = [
        jnp.pad(leaves[k].reshape(-1), (0, -leaves[k].size % width)).reshape(-1, width)
        for k in turns
    ]
    both, at, found = (lax.all_gather(jnp.concatenate(lines), axis), 0, {})
    for k, line in zip(turns, lines):
        piece = both[:, at : at + len(line)].reshape(len(both), -1)
        found[k] = piece[:, : leaves[k].size].reshape(-1, *leaves[k].shape)
        at += len(line)
    numbers = iter(range(len(leaves)))
    return jax.tree.map(lambda _: found[next(numbers)], shard)


def combined_by_axis(shard, axes, combine):
    for axis in axes:
        pieces = collected_together(shard, axis)
        shard = jax.tree.map(lambda part: part[0], pieces)
        for k in range(1, lax.axis_size(axis)):
            shard = combine(shard, jax.tree.map(lambda part: part[k], pieces))
    return shard


def cut_along(shard, dim, devices):
    shape = shard.shape
    tiles = shard.reshape(*shape[:dim], devices, shape[dim] // devices, *shape[dim + 1 :])
    return jnp.moveaxis(tiles, dim, 0)


def sent_and_summed(shard, axis, dim):
    devices = lax.axis_size(axis)
    tiles = lax.all_to_all(cut_along(shard, dim, devices), axis, 0, 0, tiled=True)
    return jnp.sum(tiles.astype(jnp.float32), axis=0)


def side_by_side(arrays, axis, dim, along):
    widths = [a.shape[along] for a in arrays]
    both = jnp.concatenate(arrays, axis=along)
    result = sent_and_summed(both, axis, dim)
    return tuple(jnp.split(result, [sum(widths[:k]) for k in range(1, len(widths))], axis=along))


def in_order(tiles, dim):
    shape = list(tiles.shape[1:])
    shape[dim] *= tiles.shape[0]
    return jnp.moveaxis(tiles, 0, dim).reshape(shape)


def gather_directly(shard, axis, dim):
    return in_order(sent_to_all(shard, axis), dim)


def combine_parts(earlier, later):
    earlier_top, earlier_total, earlier_sum = earlier
    later_top, later_total, later_sum = later
    joint_top = jnp.maximum(earlier_top, later_top)
    earlier_scale = jnp.exp(earlier_top - joint_top)
    later_scale = jnp.exp(later_top - joint_top)
    joint_total = earlier_total * earlier_scale + later_total * later_scale
    joint_sum = earlier_sum * earlier_scale[..., None] + later_sum * later_scale[..., None]
    return (joint_top, joint_total, joint_sum)


def normalize_block(mixture, norm_gain):
    row_sum, row_square = packed_total(
        (jnp.sum(mixture, axis=1), jnp.sum(mixture * mixture, axis=1)), KV
    )
    centre = row_sum / D
    spread = row_square / D - centre * centre
    scaled = (mixture - centre[:, None]) * lax.rsqrt(spread[:, None] + EPSILON) * norm_gain
    return scaled.astype(jnp.bfloat16)


def on_device(
    tokens,
    live_lengths,
    kv_cache,
    gate_sums,
    w_query,
    w_key,
    w_value,
    w_forget,
    forget_bias,
    w_out,
    first_gain,
    w_gate,
    w_up,
    w_down,
    second_gain,
):
    sequences = tokens.shape[0]
    own_cols = tokens.shape[1]
    gains_pair = jnp.stack([first_gain, second_gain], axis=0)
    wide_rows, wide_gains = gather_turned((tokens.astype(jnp.float32), gains_pair), "tp", (1, 1))
    block_rows = wide_rows.astype(jnp.bfloat16)
    row_count = block_rows.shape[1]
    row_start = lax.axis_index(KV) * row_count
    local_heads = kv_cache.shape[2] // (2 * DH)
    head_start = lax.axis_index("tp") * local_heads
    forget_rows = lax.dynamic_slice(w_forget, (row_start, head_start), (row_count, local_heads))
    query_part = jnp.dot(block_rows, w_query, preferred_element_type=jnp.float32)
    key_part = jnp.dot(block_rows, w_key, preferred_element_type=jnp.float32)
    value_part = jnp.dot(block_rows, w_value, preferred_element_type=jnp.float32)
    forget_part = jnp.dot(block_rows, forget_rows, preferred_element_type=jnp.float32)
    query_sum, key_sum, value_sum, forget_sum = packed_total(
        (query_part, key_part, value_part, forget_part), KV
    )
    queries = query_sum.astype(jnp.bfloat16).reshape(sequences, local_heads, GROUP, DH)
    new_keys = key_sum.astype(jnp.bfloat16).reshape(sequences, local_heads, DH)
    new_values = value_sum.astype(jnp.bfloat16).reshape(sequences, local_heads, DH)
    bias_rows = lax.dynamic_slice_in_dim(forget_bias, head_start, local_heads)
    new_gate = jax.nn.log_sigmoid(forget_sum + bias_rows)
    positions = kv_cache.shape[1]
    cached = kv_cache.reshape(sequences, positions, local_heads, 2, DH)
    score_scale = DH ** (-0.5)
    scores = (
        jnp.einsum(
            "bgjd,bpgd->bgjp", queries, cached[:, :, :, 0], preferred_element_type=jnp.float32
        )
        * score_scale
    )
    scores = scores + gate_sums[:, :, None, :] + new_gate[:, :, None, None]
    position_selector = lax.axis_index(KV) * positions + jnp.arange(positions, dtype=jnp.int32)
    live_mask = (position_selector[None, :] < live_lengths[:, None])[:, None, None, :]
    local_top = jnp.max(jnp.where(live_mask, scores, EMPTY_SCORE), axis=-1)
    weights = jnp.where(live_mask, jnp.exp(scores - local_top[..., None]), 0.0)
    local_total = jnp.sum(weights, axis=-1)
    local_sum = jnp.einsum(
        "bgjp,bpgd->bgjd",
        weights.astype(jnp.bfloat16),
        cached[:, :, :, 1],
        preferred_element_type=jnp.float32,
    )
    row_top, weight_total, summed = combined_by_axis(
        (local_top, local_total, local_sum), KV, combine_parts
    )
    own_score = (
        jnp.einsum("bgjd,bgd->bgj", queries, new_keys, preferred_element_type=jnp.float32)
        * score_scale
    )
    final_top = jnp.maximum(row_top, own_score)
    carry_scale = jnp.exp(row_top - final_top)
    own_weight = jnp.exp(own_score - final_top)
    own_rounded = lax.optimization_barrier(own_weight.astype(jnp.bfloat16)).astype(jnp.float32)
    numerator = summed * carry_scale[..., None] + own_rounded[..., None] * new_values[
        :, :, None, :
    ].astype(jnp.float32)
    attended = (numerator / (weight_total * carry_scale + own_weight)[..., None]).astype(
        jnp.bfloat16
    )
    attended = attended.reshape(sequences, local_heads * GROUP * DH)
    attn_part = jnp.dot(attended, w_out, preferred_element_type=jnp.float32)
    attn_block = over_copies(attn_part, "tp")
    mid_rows = normalize_block(wide_rows + attn_block, wide_gains[0])
    gate_part = jnp.dot(mid_rows, w_gate, preferred_element_type=jnp.float32)
    up_part = jnp.dot(mid_rows, w_up, preferred_element_type=jnp.float32)
    gate_share, up_share = side_by_side(
        (gate_part.astype(jnp.bfloat16), up_part.astype(jnp.bfloat16)), KV, 1, 0
    )
    hidden_share = (jax.nn.silu(gate_share) * up_share).astype(jnp.bfloat16)
    hidden = gather_directly(hidden_share, KV, 1)
    ffn_part = jnp.dot(hidden, w_down, preferred_element_type=jnp.float32)
    ffn_block = over_copies(ffn_part, "tp")
    out_block = normalize_block(mid_rows.astype(jnp.float32) + ffn_block, wide_gains[1])
    return lax.dynamic_slice_in_dim(out_block, lax.axis_index("tp") * own_cols, own_cols, 1)


def solution(mesh):
    split = Mesh(mesh.devices.reshape(8, 4, mesh.shape["tp"]), ("kv_0", "kv_1", "tp"))
    placed = (
        P(None, KV_TP),
        P(),
        P(None, KV, "tp"),
        P(None, "tp", KV),
        P(KV, "tp"),
        P(KV, "tp"),
        P(KV, "tp"),
        P(),
        P(),
        P("tp", KV),
        P(KV_TP),
        P(KV, "tp"),
        P(KV, "tp"),
        P("tp", KV),
        P(KV_TP),
    )
    return jax.shard_map(
        on_device, mesh=split, in_specs=placed, out_specs=P(None, KV_TP), check_vma=False
    )
```

profile of v0, /device:TPU:1, one launch (start us, length us, event | category | flops | bytes accessed | tf_op | source)
XLA Modules:
  0.0 193.3 jit_solution(11887656849411303763)
XLA Ops:
  0.0 0.8 maximum_bitcast_fusion.2
  0.9 0.7 convert_bitcast_fusion
  1.7 21.0 %all_gather.15 = f32[128,18]{1,0:T(8,128)S(1)} all-gather(f32[8,18]{1,0:T(8,128)S(1)} %pad_maximum_fusion.2), channel_id=1, replica_groups=mesh['kv_0'=8,'kv_1'=4,'tp'=16] {'tp'}, dimensions={0}, use_global_device_ids=true | all-gather | bytes 9792 | tf_op jit(solution)/shard_map/all_gather | solution.py:42
  22.7 0.9 fusion.70
  23.7 0.8 fusion.69
  24.6 1.0 convolution_bitcast_fusion
  25.6 0.9 convolution_bitcast_fusion.1
  26.5 1.3 broadcast_in_dim.31
  27.8 11.0 %all-to-all-start = ((f32[32,1,6160]{2,1,0:T(1,128)}), f32[32,1,6160]{2,1,0:T(1,128)S(1)}, u32[]{:S(2)}, u32[]{:S(2)}) async-start(f32[32,1,6160]{2,1,0:T(1,128)} %broadcast_in_dim.31), calls=%async_computation | async-start | bytes 1605632 | tf_op jit(solution)/shard_map/all_to_all | solution.py:20
  38.8 0.6 dynamic_slice.10
  39.4 2.6 %copy.118 = bf16[16,512,128]{1,2,0:T(8,128)(2,1)} copy(bf16[16,512,128]{2,1,0:T(8,128)(2,1)S(1)} %copy-done.1) | data formatting | bytes 4194304 | tf_op args[2]
  42.1 18.6 %all-to-all-done = f32[32,1,6160]{2,1,0:T(1,128)S(1)} async-done(((f32[32,1,6160]{2,1,0:T(1,128)}), f32[32,1,6160]{2,1,0:T(1,128)S(1)}, u32[]{:S(2)}, u32[]{:S(2)}) %all-to-all-start) | async-done | bytes 788512 | tf_op jit(solution)/shard_map/all_to_all | solution.py:20
  60.7 0.5 reduce_sum.99
  61.2 0.7 fusion.38
  61.9 1.6 select_reduce_fusion
  64.5 18.6 %all-gather.2 = f32[8,66,64]{1,2,0:T(8,128)S(1)} all-gather(f32[1,66,64]{1,2,0:T(8,128)S(1)} %maximum_bitcast_fusion), channel_id=2, replica_groups=mesh['kv_0'=8,'kv_1'=4,'tp'=16] {'kv_0'}, dimensions={0}, use_global_device_ids=true | all-gather | bytes 152064 | tf_op jit(solution)/shard_map/all_gather | solution.py:60
  83.1 0.5 slice_reduce_fusion.25
  84.1 10.5 %all-gather.3 = f32[4,66,64]{1,2,0:T(8,128)S(1)} all-gather(f32[1,66,64]{1,2,0:T(8,128)S(1)} %maximum_bitcast_fusion.1), channel_id=3, replica_groups=mesh['kv_0'=8,'kv_1'=4,'tp'=16] {'kv_1'}, dimensions={0}, use_global_device_ids=true | all-gather | bytes 84480 | tf_op jit(solution)/shard_map/all_gather | solution.py:60
  98.6 0.7 broadcast_in_dim.34
  99.2 14.6 %all-to-all-start.1 = ((f32[16,16,128]{2,1,0:T(8,128)}), f32[16,16,128]{2,1,0:T(8,128)S(1)}, u32[]{:S(2)}, u32[]{:S(2)}) async-start(f32[16,16,128]{2,1,0:T(8,128)} %broadcast_in_dim.34), calls=%async_computation.1 | async-start | bytes 262144 | tf_op jit(solution)/shard_map/all_to_all | solution.py:20
  113.9 8.8 %all-to-all-done.1 = f32[16,16,128]{2,1,0:T(8,128)S(1)} async-done(((f32[16,16,128]{2,1,0:T(8,128)}), f32[16,16,128]{2,1,0:T(8,128)S(1)}, u32[]{:S(2)}, u32[]{:S(2)}) %all-to-all-start.1) | async-done | bytes 131104 | tf_op jit(solution)/shard_map/all_to_all | solution.py:20
  122.9 0.6 broadcast_in_dim.35
  123.5 5.3 %all-to-all-start.2 = ((f32[32,1,32]{2,1,0:T(1,128)}), f32[32,1,32]{2,1,0:T(1,128)S(1)}, u32[]{:S(2)}, u32[]{:S(2)}) async-start(f32[32,1,32]{2,1,0:T(1,128)} %broadcast_in_dim.35), calls=%async_computation.2 | async-start | bytes 32768 | tf_op jit(solution)/shard_map/all_to_all | solution.py:20
  129.1 8.4 %all-to-all-done.2 = f32[32,1,32]{2,1,0:T(1,128)S(1)} async-done(((f32[32,1,32]{2,1,0:T(1,128)}), f32[32,1,32]{2,1,0:T(1,128)S(1)}, u32[]{:S(2)}, u32[]{:S(2)}) %all-to-all-start.2) | async-done | bytes 4128 | tf_op jit(solution)/shard_map/all_to_all | solution.py:20
  138.1 0.6 reshape.1443
  139.3 11.7 %all_to_all.38 = bf16[32,2,352]{2,1,0:T(2,128)(2,1)S(1)} all-to-all(bf16[32,2,352]{2,1,0:T(2,128)(2,1)S(1)} %reshape.1497), channel_id=1, replica_groups=mesh['kv_0'=8,'kv_1'=4,'tp'=16] {'kv_0','kv_1'}, dimensions={0} | all-to-all | bytes 90112 | tf_op jit(solution)/shard_map/all_to_all | solution.py:86
  151.8 11.7 %all_to_all.39 = bf16[32,2,176]{2,1,0:T(2,128)(2,1)S(1)} all-to-all(bf16[32,2,176]{2,1,0:T(2,128)(2,1)S(1)} %reshape.1499), channel_id=1, replica_groups=mesh['kv_0'=8,'kv_1'=4,'tp'=16] {'kv_0','kv_1'}, dimensions={0} | all-to-all | bytes 45056 | tf_op jit(solution)/shard_map/all_to_all | solution.py:20
  164.0 15.1 %all_to_all.40 = f32[16,16,128]{2,1,0:T(8,128)S(1)} all-to-all(f32[16,16,128]{2,1,0:T(8,128)S(1)} %broadcast_in_dim.37), channel_id=1, replica_groups=mesh['kv_0'=8,'kv_1'=4,'tp'=16] {'tp'}, dimensions={0} | all-to-all | bytes 262144 | tf_op jit(solution)/shard_map/all_to_all | solution.py:20
  179.3 0.6 broadcast_in_dim.38
  179.9 3.9 %all-to-all-start.6 = ((f32[32,1,32]{2,1,0:T(1,128)}), f32[32,1,32]{2,1,0:T(1,128)S(1)}, u32[]{:S(2)}, u32[]{:S(2)}) async-start(f32[32,1,32]{2,1,0:T(1,128)} %broadcast_in_dim.38), calls=%async_computation.6 | async-start | bytes 32768 | tf_op jit(solution)/shard_map/all_to_all | solution.py:20
  183.9 8.5 %all-to-all-done.6 = f32[32,1,32]{2,1,0:T(1,128)S(1)} async-done(((f32[32,1,32]{2,1,0:T(1,128)}), f32[32,1,32]{2,1,0:T(1,128)S(1)}, u32[]{:S(2)}, u32[]{:S(2)}) %all-to-all-start.6) | async-done | bytes 4128 | tf_op jit(solution)/shard_map/all_to_all | solution.py:20
  192.6 0.7 copy.138
  (126 shorter events, 9.1 us)
Async XLA Ops:
  0.0 137.7 %copy-start = (bf16[128,704]{0,1:T(8,128)(2,1)S(1)}, bf16[128,704]{0,1:T(8,128)(2,1)}, u32[]{:S(2)}) copy-start(bf16[128,704]{0,1:T(8,128)(2,1)} %param.27) | copy-start | bytes 540676
  0.0 38.8 %copy-start.8 = (f32[16]{0:T(128)S(1)}, f32[16]{0:T(128)}, u32[]{:S(2)}) copy-start(f32[16]{0:T(128)} %param.23) | copy-start | bytes 196
  0.0 39.4 %copy-start.6 = (f32[16,1,512]{2,1,0:T(1,128)S(1)}, f32[16,1,512]{2,1,0:T(1,128)}, u32[]{:S(2)}) copy-start(f32[16,1,512]{2,1,0:T(1,128)} %param.18) | copy-start | bytes 98308
  0.0 39.4 %copy-start.1 = (bf16[16,512,128]{2,1,0:T(8,128)(2,1)S(1)}, bf16[16,512,128]{2,1,0:T(8,128)(2,1)}, u32[]{:S(2)}) copy-start(bf16[16,512,128]{2,1,0:T(8,128)(2,1)} %param.17) | copy-start | bytes 6291460
  27.8 32.9 %all-to-all-start = ((f32[32,1,6160]{2,1,0:T(1,128)}), f32[32,1,6160]{2,1,0:T(1,128)S(1)}, u32[]{:S(2)}, u32[]{:S(2)}) async-start(f32[32,1,6160]{2,1,0:T(1,128)} %broadcast_in_dim.31), calls=%async_computation | async-start | bytes 1605632 | tf_op jit(solution)/shard_map/all_to_all | solution.py:20
  39.4 2.6 %copy-start.7 = (s32[16]{0:T(128)S(1)}, s32[16]{0:T(128)}, u32[]{:S(2)}) copy-start(s32[16]{0:T(128)} %param.16) | copy-start | bytes 196
  42.0 21.5 %copy-start.2 = (bf16[16,512,128]{1,2,0:T(8,128)(2,1)S(1)}, bf16[16,512,128]{1,2,0:T(8,128)(2,1)}, u32[]{:S(2)}) copy-start(bf16[16,512,128]{1,2,0:T(8,128)(2,1)} %copy.118) | copy-start | bytes 6291460
  63.9 34.5 %copy-start.5 = (bf16[256,128]{1,0:T(8,128)(2,1)S(1)}, bf16[256,128]{1,0:T(8,128)(2,1)}, u32[]{:S(2)}) copy-start(bf16[256,128]{1,0:T(8,128)(2,1)} %param.24) | copy-start | bytes 196612
  84.0 53.9 %copy-start.3 = (bf16[128,704]{0,1:T(8,128)(2,1)S(1)}, bf16[128,704]{0,1:T(8,128)(2,1)}, u32[]{:S(2)}) copy-start(bf16[128,704]{0,1:T(8,128)(2,1)} %param.26) | copy-start | bytes 540676
  98.6 65.3 %copy-start.4 = (bf16[704,128]{1,0:T(8,128)(2,1)S(1)}, bf16[704,128]{1,0:T(8,128)(2,1)}, u32[]{:S(2)}) copy-start(bf16[704,128]{1,0:T(8,128)(2,1)} %param.28) | copy-start | bytes 540676
  99.2 23.5 %all-to-all-start.1 = ((f32[16,16,128]{2,1,0:T(8,128)}), f32[16,16,128]{2,1,0:T(8,128)S(1)}, u32[]{:S(2)}, u32[]{:S(2)}) async-start(f32[16,16,128]{2,1,0:T(8,128)} %broadcast_in_dim.34), calls=%async_computation.1 | async-start | bytes 262144 | tf_op jit(solution)/shard_map/all_to_all | solution.py:20
  123.5 14.0 %all-to-all-start.2 = ((f32[32,1,32]{2,1,0:T(1,128)}), f32[32,1,32]{2,1,0:T(1,128)S(1)}, u32[]{:S(2)}, u32[]{:S(2)}) async-start(f32[32,1,32]{2,1,0:T(1,128)} %broadcast_in_dim.35), calls=%async_computation.2 | async-start | bytes 32768 | tf_op jit(solution)/shard_map/all_to_all | solution.py:20
  179.9 12.5 %all-to-all-start.6 = ((f32[32,1,32]{2,1,0:T(1,128)}), f32[32,1,32]{2,1,0:T(1,128)S(1)}, u32[]{:S(2)}, u32[]{:S(2)}) async-start(f32[32,1,32]{2,1,0:T(1,128)} %broadcast_in_dim.38), calls=%async_computation.6 | async-start | bytes 32768 | tf_op jit(solution)/shard_map/all_to_all | solution.py:20
where the time goes:
time: 194 us; the launch traced here: 193 us
  blocking collectives  88.6 us (46%)
  waiting for transfers between devices  44.4 us (23%)
  starting transfers between devices  34.8 us (18%)
  local copies, waits for them, and re-layouts  14.5 us (7%)
  matrix products  6.3 us (3%)
  other arithmetic  4.36 us (2%)
    all_to_all x4, waiting for transfers between devices, sent_to_all(): lax.all_to_all(jnp.broadcast_to(shard[None], (devices, *shard.shape)), ax...  44.4 us
    all_to_all x4, starting transfers between devices, sent_to_all(): lax.all_to_all(jnp.broadcast_to(shard[None], (devices, *shard.shape)), ax...  34.8 us
    all_gather x2, blocking collectives, collected_together(): both, at, found = (lax.all_gather(jnp.concatenate(lines), axis), 0, {})  29.2 us
    all_to_all x2, blocking collectives, sent_to_all(): lax.all_to_all(jnp.broadcast_to(shard[None], (devices, *shard.shape)), ax...  26.8 us
    all_gather x1, blocking collectives, gather_turned(): result = lax.all_gather(both, axis, axis=0, tiled=True)  21 us
    all_to_all x1, blocking collectives, sent_and_summed(): lax.all_to_all(cut_along(shard, dim, devices), axis, 0, 0, tiled=True)  11.7 us
  transfers between devices with their start and end apart: 4, of which 4 were waited for; matrix products, arithmetic and copies ran while one was open for 2% of the time, Pallas kernels for 0%

commit v1 on v0

v1 whole, which is shorter than its diff:
```python
import jax
import jax.numpy as jnp
from jax import lax
from jax.experimental import pallas as pl
from jax.experimental.pallas import tpu as pltpu
from jax.sharding import PartitionSpec as P

MESH = pl.DeviceIdType.MESH
F32 = jnp.float32
BF16 = jnp.bfloat16

D = 4096
DH = 64
B = 16
X = 4
Z = 8
KV = 32
TP = 16
POS = 512
UNITS = 704
WIDE = 768
EPSILON = 1e-05
EMPTY_SCORE = -1e30
NT = (((1,), (1,)), ((), ()))


def iota(shape, dim):
    return lax.broadcasted_iota(jnp.int32, shape, dim)


def split3(v):
    hi = v.astype(BF16).astype(F32)
    rest = v - hi
    mid = rest.astype(BF16).astype(F32)
    return hi, mid, rest - mid


def nt(a, b):
    return lax.dot_general(a, b, NT, preferred_element_type=F32)


def lane_sum(v, lo, hi):
    lane = iota(v.shape, 1)
    return jnp.sum(jnp.where((lane >= lo) & (lane < hi), v, 0.0), axis=1, keepdims=True)


def kernel(
    lengths, bias, tok, g1, g2, kv_hbm, gs_hbm, wq_hbm, wk_hbm, wv_hbm, wf_hbm, wo_hbm, wg_hbm,
    wu_hbm, wd_hbm, out,
    cache, gs, wq, wkv, wf, wo, wg, wu, wd,
    tokv, gainv,
    b1, qx, qz, kx, kz, ax, az, b4, gm, bg, m5, b5, b6, b7, b8,
    qs, ngs, osum, otop, otot, pbuf, sbuf, gbuf,
    lsem, ssem, rsem,
):
    kv = lax.axis_index("kv")
    tp = lax.axis_index("tp")
    x = lax.rem(kv, X)
    z = kv // X

    loads = []

    def load(src, dst):
        c = pltpu.make_async_copy(src, dst, lsem.at[len(loads)])
        c.start()
        loads.append(c)
        return c

    l_tok = load(tok, tokv)
    l_g1 = load(g1, gainv.at[0])
    l_g2 = load(g2, gainv.at[1])
    l_wq = load(wq_hbm, wq)
    l_wk = load(wk_hbm, wkv.at[pl.ds(0, DH)])
    l_wv = load(wv_hbm, wkv.at[pl.ds(DH, DH)])
    l_wf = load(wf_hbm.at[:, pl.ds(pl.multiple_of(kv * 128, 128), 128)], wf)
    l_gs = load(gs_hbm, gs)
    l_kv = load(kv_hbm, cache)
    l_wg = load(wg_hbm, wg)
    l_wu = load(wu_hbm, wu)
    l_wo = load(wo_hbm, wo)
    l_wd = load(wd_hbm, wd.at[pl.ds(0, UNITS)])

    def kv_peer(i):
        a = lax.rem(kv + i, KV)
        return a, (a, tp)

    def x_peer(i):
        a = z * X + lax.rem(x + i, X)
        return a, (a, tp)

    def z_peer(i):
        a = lax.rem(kv + X * i, KV)
        return a, (a, tp)

    def tp_peer(i):
        a = lax.rem(tp + i, TP)
        return a, (kv, a)

    bar = pltpu.get_barrier_semaphore()

    def signal_kv(i, c):
        pl.semaphore_signal(bar, inc=1, device_id=kv_peer(i)[1], device_id_type=MESH)
        return c

    def signal_tp(i, c):
        pl.semaphore_signal(bar, inc=1, device_id=tp_peer(i)[1], device_id_type=MESH)
        return c

    lax.fori_loop(1, KV, signal_kv, 0)
    lax.fori_loop(1, TP, signal_tp, 0)

    waits = []
    used = [0]

    def exchange(n, peer, src_of, buf, slot):
        k = used[0]
        used[0] += 1

        def send(i, c):
            a, dev = peer(i)
            pltpu.make_async_remote_copy(
                src_ref=src_of(a), dst_ref=buf.at[slot], send_sem=ssem.at[k],
                recv_sem=rsem.at[k], device_id=dev, device_id_type=MESH,
            ).start()
            return c

        lax.fori_loop(1, n, send, 0, unroll=True)
        some = buf.at[pl.ds(0, n - 1)]
        waits.append(pltpu.make_async_copy(some, some, ssem.at[k]))
        return pltpu.make_async_copy(some, some, rsem.at[k])

    def spread(n, peer, buf, slot):
        return exchange(n, peer, lambda a: buf.at[slot], buf, slot)

    wd[pl.ds(UNITS, WIDE - UNITS), :] = jnp.zeros((WIDE - UNITS, 128), BF16)
    pbuf[...] = jnp.zeros_like(pbuf)
    gbuf[...] = jnp.zeros_like(gbuf)
    sbuf[...] = jnp.zeros_like(sbuf)
    gm[...] = jnp.zeros_like(gm)

    l_tok.wait()
    l_g1.wait()
    l_g2.wait()
    lane8 = iota((8, 128), 1)
    diag8 = iota((8, 8), 0) == iota((8, 8), 1)
    c1 = jnp.sum(jnp.where(diag8, gainv[0], 0.0), axis=1, keepdims=True)
    c2 = jnp.sum(jnp.where(diag8, gainv[1], 0.0), axis=1, keepdims=True)
    b1[tp] = jnp.where(lane8 == 16, c1, jnp.where(lane8 == 17, c2, 0.0))
    b1[tp, :, 0:B] = tokv[...].astype(F32)
    pl.semaphore_wait(bar, KV - 1 + TP - 1)
    r1 = spread(TP, tp_peer, b1, tp)
    l_wq.wait()
    l_wk.wait()
    l_wv.wait()
    l_wf.wait()
    r1.wait()
    turned = jnp.transpose(b1[...].reshape(128, 128))
    rows = turned[0:B, :]
    gain1 = turned[B : B + 1, :]
    gain2 = turned[B + 1 : B + 2, :]
    rows16 = rows.astype(BF16)

    lane = iota((B, 128), 1)
    q_part = jnp.dot(rows16, wq[...], preferred_element_type=F32)
    f_all = nt(rows16, wf[...])
    f_part = jnp.sum(jnp.where(iota((B, B), 1) == tp, f_all, 0.0), axis=1, keepdims=True)
    t_part = jnp.sum(rows, axis=1, keepdims=True)

    def small_tile(first, second):
        tile = jnp.zeros((B, 128), F32)
        for k, piece in enumerate((*split3(first), *split3(second))):
            tile = jnp.where(lane == k, piece, tile)
        return tile

    qx[x, 0:B] = q_part[:, 0:128].astype(BF16)
    qx[x, B : 2 * B] = q_part[:, 128:256].astype(BF16)
    qx[x, 2 * B : 3 * B] = small_tile(f_part, t_part).astype(BF16)
    r = spread(X, x_peer, qx, x)
    kx[x] = nt(rows16, wkv[...]).astype(BF16)
    rk = spread(X, x_peer, kx, x)
    r.wait()
    summed = jnp.sum(qx[...].astype(F32), axis=0)
    small = summed[2 * B : 3 * B]
    qz[z, 0 : 2 * B] = summed[0 : 2 * B].astype(BF16)
    qz[z, 2 * B : 3 * B] = small_tile(lane_sum(small, 0, 3), lane_sum(small, 3, 6)).astype(BF16)
    r = spread(Z, z_peer, qz, z)
    rk.wait()
    kz[z] = jnp.sum(kx[...].astype(F32), axis=0).astype(BF16)
    rk = spread(Z, z_peer, kz, z)

    l_wg.wait()
    l_wu.wait()
    row16 = iota((B, 128), 0)
    gh, gmid, gl = split3(gain1)
    gain_rows = jnp.where(
        row16 == 0, gh, jnp.where(row16 == 1, gmid, jnp.where(row16 == 2, gl, 0.0))
    ).astype(BF16)
    gbuf[0:1, 0:UNITS] = jnp.sum(nt(gain_rows, wg[...]), axis=0, keepdims=True)
    gbuf[1:2, 0:UNITS] = jnp.sum(nt(gain_rows, wu[...]), axis=0, keepdims=True)
    for h in range(2):
        for t in range(3):
            at = (h * 3 + t) * 128
            gm[h, t : t + 1, :] = gbuf[0:1, at : at + 128]
            gm[h, 3 + t : 4 + t, :] = gbuf[1:2, at : at + 128]
    half = lax.rem(kv, 2)
    bg[kv] = gm[half]
    l_gs.wait()
    l_kv.wait()

    r.wait()
    summed = jnp.sum(qz[...].astype(F32), axis=0)
    q0 = summed[0:B].astype(BF16).astype(F32)
    q1 = summed[B : 2 * B].astype(BF16).astype(F32)
    small = summed[2 * B : 3 * B]
    tok_mean = lane_sum(small, 3, 6) * (1.0 / D)
    gate_in = lane_sum(small, 0, 3) + bias[tp]
    new_gate = jnp.minimum(gate_in, 0.0) - jnp.log1p(jnp.exp(-jnp.abs(gate_in)))
    rg = exchange(KV, kv_peer, lambda a: gm.at[lax.rem(a, 2)], bg, kv)

    low = lane < DH
    qs[pl.ds(0, B, stride=4), :] = jnp.where(low, q0, 0.0)
    qs[pl.ds(1, B, stride=4), :] = jnp.where(low, pltpu.roll(q0, DH, 1), 0.0)
    qs[pl.ds(2, B, stride=4), :] = jnp.where(low, q1, 0.0)
    qs[pl.ds(3, B, stride=4), :] = jnp.where(low, pltpu.roll(q1, DH, 1), 0.0)
    gate_tile = jnp.broadcast_to(new_gate, (B, 128))
    for j in range(4):
        ngs[pl.ds(j, B, stride=4), :] = gate_tile
    scale = DH ** (-0.5)
    first = iota((8, POS), 0) < 4
    first128 = iota((8, 128), 0) < 4
    position = iota((8, POS), 1) + kv * POS
    for p in range(B // 2):
        own = pl.ds(8 * p, 8)
        queries = qs[own, :].astype(BF16)
        s = jnp.where(first, nt(queries, cache[2 * p]), nt(queries, cache[2 * p + 1])) * scale
        s = s + jnp.where(first, gs[2 * p], gs[2 * p + 1]) + ngs[own, 0:1]
        live = position < jnp.where(first, lengths[2 * p], lengths[2 * p + 1])
        top = jnp.max(jnp.where(live, s, EMPTY_SCORE), axis=1, keepdims=True)
        w = jnp.where(live, jnp.exp(s - top), 0.0)
        w16 = w.astype(BF16)
        osum[own, :] = jnp.where(
            first128,
            jnp.dot(w16, cache[2 * p], preferred_element_type=F32),
            jnp.dot(w16, cache[2 * p + 1], preferred_element_type=F32),
        )
        otop[own, :] = jnp.broadcast_to(top, (8, 128))
        otot[own, :] = jnp.broadcast_to(jnp.sum(w, axis=1, keepdims=True), (8, 128))

    def by_head(ref):
        return [ref[pl.ds(j, B, stride=4), :] for j in range(4)]

    os, tops, tots = by_head(osum), by_head(otop), by_head(otot)
    sums = [jnp.where(low, pltpu.roll(os[2 * i], DH, 1), os[2 * i + 1]) for i in range(2)]
    tops = [jnp.where(low, tops[2 * i], tops[2 * i + 1]) for i in range(2)]
    tots = [jnp.where(low, tots[2 * i], tots[2 * i + 1]) for i in range(2)]

    place = lax.rem(lane, DH)

    def pack(buf, slot):
        buf[slot, 0:B] = sums[0].astype(BF16)
        buf[slot, B : 2 * B] = sums[1].astype(BF16)
        tile = jnp.zeros((B, 128), F32)
        k = 0
        for v in (*tops, *tots):
            for piece in split3(v):
                tile = jnp.where(place == k, piece, tile)
                k += 1
        buf[slot, 2 * B : 3 * B] = tile.astype(BF16)

    src = iota((128, 512), 0)
    dst = iota((128, 512), 1)
    wanted = 3 * (dst // 128)
    pick = (src // DH == lax.rem(dst, 128) // DH) & (lax.rem(src, DH) >= wanted)
    pick = jnp.where(pick & (lax.rem(src, DH) < wanted + 3), 1.0, 0.0).astype(BF16)

    def unpack(buf, n):
        spreads = [
            jnp.dot(buf[i, 2 * B : 3 * B], pick, preferred_element_type=F32) for i in range(n)
        ]
        new_sums, new_tops, new_tots = [], [], []
        for c in range(2):
            t = [v[:, c * 128 : c * 128 + 128] for v in spreads]
            u = [v[:, 256 + c * 128 : 384 + c * 128] for v in spreads]
            top = t[0]
            for v in t[1:]:
                top = jnp.maximum(top, v)
            total, weighted = 0.0, 0.0
            for i in range(n):
                e = jnp.exp(t[i] - top)
                total = total + u[i] * e
                weighted = weighted + buf[i, c * B : c * B + B].astype(F32) * e
            new_sums.append(weighted)
            new_tops.append(top)
            new_tots.append(total)
        return new_sums, new_tops, new_tots

    pack(ax, x)
    r = spread(X, x_peer, ax, x)
    rk.wait()
    keyval = jnp.sum(kz[...].astype(F32), axis=0).astype(BF16).astype(F32)
    turned_kv = pltpu.roll(keyval, DH, 1)
    keys = jnp.where(low, keyval, turned_kv)
    values = jnp.where(low, turned_kv, keyval)
    owns = []
    for q in (q0, q1):
        prod = q * keys
        owns.append(jnp.where(low, lane_sum(prod, 0, DH), lane_sum(prod, DH, 128)) * scale)
    r.wait()
    sums, tops, tots = unpack(ax, X)
    pack(az, z)
    r = spread(Z, z_peer, az, z)
    rg.wait()
    gained = jnp.sum(bg[...], axis=0)
    l_wo.wait()
    r.wait()
    sums, tops, tots = unpack(az, Z)
    attended = []
    for c in range(2):
        final = jnp.maximum(tops[c], owns[c])
        carry = jnp.exp(tops[c] - final)
        own_weight = jnp.exp(owns[c] - final)
        top_part = sums[c] * carry + own_weight.astype(BF16).astype(F32) * values
        attended.append((top_part / (tots[c] * carry + own_weight)).astype(BF16))

    proj = jnp.dot(attended[0], wo[0:128, :], preferred_element_type=F32)
    proj = proj + jnp.dot(attended[1], wo[128:256, :], preferred_element_type=F32)
    b4[tp] = proj.astype(BF16)
    r = spread(TP, tp_peer, b4, tp)
    r.wait()
    centred = rows + jnp.sum(b4[...].astype(F32), axis=0) - tok_mean

    gained_rows = (centred * gain1).astype(BF16)
    stat = small_tile(
        jnp.sum(centred, axis=1, keepdims=True), jnp.sum(centred * centred, axis=1, keepdims=True)
    )
    for h in range(2):
        sbuf[pl.ds(h * 8 + 6, B, stride=16), :] = stat
    for which, w in enumerate((wg, wu)):
        pbuf[which, :, 0:UNITS] = nt(gained_rows, w[...])
        for h in range(2):
            for t in range(3):
                at = (h * 3 + t) * 128
                sbuf[pl.ds(h * 8 + which * 3 + t, B, stride=16), :] = pbuf[which, :, at : at + 128]
    m5[...] = sbuf[...].reshape(KV, 8, 128).astype(BF16)
    b5[kv] = m5[kv]
    r = exchange(KV, kv_peer, lambda a: m5.at[a], b5, kv)
    r.wait()
    units = jnp.sum(b5[...].astype(F32), axis=0)
    lane_row = iota((1, 128), 1)
    srow = units[6:7, :]
    mean = lane_sum(srow, 0, 3) * (1.0 / D)
    spread1 = lane_sum(srow, 3, 6) * (1.0 / D) - mean * mean
    rstd = lax.rsqrt(spread1 + EPSILON)
    units = (units - mean * gained) * rstd
    gates = units[0:3, :]
    hidden = gates / (1.0 + jnp.exp(-gates)) * units[3:6, :]
    b6[kv, 0:3, :] = hidden
    b6[kv, 3:4, :] = jnp.where(lane_row == 0, mean, jnp.where(lane_row == 1, rstd, 0.0))
    r = spread(KV, kv_peer, b6, kv)
    l_wd.wait()
    r.wait()
    flat = b6.reshape(KV * 4, 128)
    tiles = [
        flat[pl.ds(h * 4 + t, B, stride=8), :].astype(BF16) for h in range(2) for t in range(3)
    ]
    norms = flat[pl.ds(3, B, stride=8), :]
    down = jnp.dot(jnp.concatenate(tiles, axis=1), wd[...], preferred_element_type=F32)

    b7[tp] = down.astype(BF16)
    r = spread(TP, tp_peer, b7, tp)
    mid = (centred - lane_sum(norms, 0, 1)) * lane_sum(norms, 1, 2) * gain1
    mid = mid.astype(BF16).astype(F32)
    r.wait()
    mixed = mid + jnp.sum(b7[...].astype(F32), axis=0)

    sum2 = jnp.sum(mixed, axis=1, keepdims=True)
    off = mixed - sum2 * (1.0 / 128)
    square2 = jnp.sum(off * off, axis=1, keepdims=True)
    stat = jnp.where(lane == row16, sum2, jnp.where(lane == row16 + B, square2, 0.0))
    b8[kv] = jnp.sum(stat, axis=0, keepdims=True)
    r = spread(KV, kv_peer, b8, kv)
    r.wait()
    stats = b8[...].reshape(KV, 128)
    total2 = jnp.sum(stats, axis=0, keepdims=True)
    drift = stats * (1.0 / 128) - total2 * (1.0 / D)
    between = jnp.sum(drift * drift, axis=0, keepdims=True) * 128.0
    mean2 = jnp.sum(jnp.where(lane == row16, total2, 0.0), axis=1, keepdims=True) * (1.0 / D)
    var2 = jnp.sum(
        jnp.where(lane == row16, between, jnp.where(lane == row16 + B, total2, 0.0)),
        axis=1, keepdims=True,
    ) * (1.0 / D)
    result = ((mixed - mean2) * lax.rsqrt(var2 + EPSILON) * gain2).astype(BF16)
    chosen = jnp.where(iota((8, 128), 1) == iota((8, 128), 0) + tp * 8, 1.0, 0.0).astype(BF16)
    out[...] = nt(chosen, result).astype(BF16)
    for w in waits:
        w.wait()


def on_device(
    tokens, live_lengths, kv_cache, gate_sums, w_query, w_key, w_value, w_forget, forget_bias,
    w_out, first_gain, w_gate, w_up, w_down, second_gain,
):
    smem = pl.BlockSpec(memory_space=pltpu.SMEM)
    hbm = pl.BlockSpec(memory_space=pl.ANY)
    vmem = pltpu.VMEM
    turned = pl.pallas_call(
        kernel,
        out_shape=jax.ShapeDtypeStruct((8, B), BF16),
        in_specs=[smem, smem] + [hbm] * 13,
        out_specs=pl.BlockSpec(memory_space=pltpu.VMEM),
        scratch_shapes=[
            vmem((B, POS, 128), BF16),
            vmem((B, 1, POS), F32),
            vmem((128, 256), BF16),
            vmem((128, 128), BF16),
            vmem((16, 128), BF16),
            vmem((256, 128), BF16),
            vmem((UNITS, 128), BF16),
            vmem((UNITS, 128), BF16),
            vmem((WIDE, 128), BF16),
            vmem((8, B), BF16),
            vmem((2, 1, 8), F32),
            vmem((TP, 8, 128), F32),
            vmem((X, 3 * B, 128), BF16),
            vmem((Z, 3 * B, 128), BF16),
            vmem((X, B, 128), BF16),
            vmem((Z, B, 128), BF16),
            vmem((X, 3 * B, 128), BF16),
            vmem((Z, 3 * B, 128), BF16),
            vmem((TP, B, 128), BF16),
            vmem((2, 8, 128), F32),
            vmem((KV, 8, 128), F32),
            vmem((KV, 8, 128), BF16),
            vmem((KV, 8, 128), BF16),
            vmem((KV, 4, 128), F32),
            vmem((TP, B, 128), BF16),
            vmem((KV, 1, 128), F32),
            vmem((64, 128), F32),
            vmem((64, 128), F32),
            vmem((64, 128), F32),
            vmem((64, 128), F32),
            vmem((64, 128), F32),
            vmem((2, B, WIDE), F32),
            vmem((KV * 8, 128), F32),
            vmem((2, WIDE), F32),
            pltpu.SemaphoreType.DMA((13,)),
            pltpu.SemaphoreType.DMA((13,)),
            pltpu.SemaphoreType.DMA((13,)),
        ],
        compiler_params=pltpu.CompilerParams(collective_id=0, has_side_effects=True),
    )(
        live_lengths, forget_bias, tokens.T, first_gain.reshape(1, 8), second_gain.reshape(1, 8),
        kv_cache, gate_sums, w_query, w_key.T, w_value.T, w_forget.T, w_out, w_gate.T, w_up.T,
        w_down,
    )
    return turned.T


def solution(mesh):
    placed = (
        P(None, ("kv", "tp")), P(), P(None, "kv", "tp"), P(None, "tp", "kv"), P("kv", "tp"),
        P("kv", "tp"), P("kv", "tp"), P(), P(), P("tp", "kv"), P(("kv", "tp")), P("kv", "tp"),
        P("kv", "tp"), P("tp", "kv"), P(("kv", "tp")),
    )
    return jax.shard_map(
        on_device, mesh=mesh, in_specs=placed, out_specs=P(None, ("kv", "tp")), check_vma=False
    )
```

time: 194 us -> 73.8 us (0.38)
  blocking collectives: 88.6 us -> 0 us
  Pallas kernels: 0 us -> 72.4 us
  waiting for transfers between devices: 44.4 us -> 0 us
  starting transfers between devices: 34.8 us -> 0 us
  local copies, waits for them, and re-layouts: 14.5 us -> 1.26 us
  matrix products: 6.3 us -> 0 us
  other arithmetic: 4.36 us -> 0 us
    pallas_call x0 -> x1, Pallas kernels: none -> 72.4 us  [on_device(): pl.pallas_call(kernel, out_shape=jax.ShapeDtypeStruct((8, B), BF16), in_s...]
    all_gather x3 -> x0, blocking collectives: 50.1 us -> none  [the longest x2 29.2 us: collected_together(): both, at, found = (lax.all_gather(jnp.concatenate(lines), axis), 0, {})]
    all_to_all x4 -> x0, waiting for transfers between devices: 44.4 us -> none  [sent_to_all(): lax.all_to_all(jnp.broadcast_to(shard[None], (devices, *shard.shape)), ax...]
    all_to_all x3 -> x0, blocking collectives: 38.5 us -> none  [the longest x2 26.8 us: sent_to_all(): lax.all_to_all(jnp.broadcast_to(shard[None], (devices, *shard.shape)), ax...]
    all_to_all x4 -> x0, starting transfers between devices: 34.8 us -> none  [sent_to_all(): lax.all_to_all(jnp.broadcast_to(shard[None], (devices, *shard.shape)), ax...]
    dot_general x11 -> x0, matrix products: 6.3 us -> none  [the longest x1 1.56 us: on_device(): jnp.einsum('bgjd,bpgd->bgjp', queries, cached[:, :, :, 0], preferred_elem...]
    broadcast_in_dim x6 -> x0, local copies, waits for them, and re-layouts: 3.26 us -> none  [sent_to_all(): jnp.broadcast_to(shard[None], (devices, *shard.shape))]
    unnamed x28 -> x1, local copies, waits for them, and re-layouts: 3.53 us -> 1.26 us
  transfers between devices with their start and end apart: 4 -> 0, of which waited for: 4 -> 0; matrix products, arithmetic and copies ran while one was open for 2% -> 0% of each run, Pallas kernels for 0% -> 0%
where the time goes in v1:
time: 73.8 us; the launch traced here: 73.7 us
  Pallas kernels  72.4 us (98%)
  local copies, waits for them, and re-layouts  1.26 us (2%)
    pallas_call x1, Pallas kernels, on_device(): pl.pallas_call(kernel, out_shape=jax.ShapeDtypeStruct((8, B), BF16), in_s...  72.4 us

profile of v1, /device:TPU:1, one launch (start us, length us, event | category | flops | bytes accessed | tf_op | source)
XLA Modules:
  0.0 73.7 jit_solution(17297347197807484636)
XLA Ops:
  0.0 72.4 %shard_map.145 = bf16[8,16]{1,0:T(8,128)(2,1)} custom-call(s32[16]{0:T(128)} %lengths.1, f32[16]{0:T(128)} %bias.1, bf16[8,16]{1,0:T(8,128)(2,1)} %bitcast.15, f32[1,8]{1,0:T(1,128)} %bitcast.16, f32[1,8]{1,0:T(1,128)} %bitcast.17, bf16[16,512,128]{2,1,0:T(8,128)(2,1)} %kv_hbm.1, f32[16,1,512]{2,1,0:T(1,128)} %gs_hbm.1, bf16[128,256]{1,0:T(8,128)(2,1)} %wq_hbm.1, ...), custom_call_target="tpu_custom_call" | custom-call | tf_op jit(solution)/shard_map/pallas_call | solution.py:406
  72.4 1.3 %copy.17 = bf16[16,8]{0,1:T(8,128)(2,1)} copy(bf16[16,8]{0,1:T(8,128)(2,1)} %bitcast.14) | data formatting | bytes 512

commit v2 on v1

--- a/solution.py
+++ b/solution.py
@@ -21,6 +21,21 @@
 WIDE = 768
 EPSILON = 1e-05
 EMPTY_SCORE = -1e30
+
+
+def hops(o, sizes):
+    return sum(min(d, n - d) for d, n in zip(o, sizes))
+
+
+def far_first(sizes):
+    offsets = [(i, j) for i in range(sizes[0]) for j in range(sizes[1]) if i or j]
+    return sorted(offsets, key=lambda o: -hops(o, sizes))
+
+
+X_FAR = [2, 1, 3]
+Z_FAR = [4, 3, 5, 2, 6, 1, 7]
+KV_FAR = far_first((Z, X))
+TP_FAR = far_first((TP // 2, 2))
 NT = (((1,), (1,)), ((), ()))
 
 
@@ -45,19 +60,41 @@
 
 
 def kernel(
-    lengths, bias, tok, g1, g2, kv_hbm, gs_hbm, wq_hbm, wk_hbm, wv_hbm, wf_hbm, wo_hbm, wg_hbm,
+    lengths_hbm, bias_hbm, tok, g1, g2, kv_hbm, gs_hbm, wq_hbm, wk_hbm, wv_hbm, wf_hbm, wo_hbm, wg_hbm,
     wu_hbm, wd_hbm, out,
     cache, gs, wq, wkv, wf, wo, wg, wu, wd,
     tokv, gainv,
     b1, qx, qz, kx, kz, ax, az, b4, gm, bg, m5, b5, b6, b7, b8,
-    qs, ngs, osum, otop, otot, pbuf, sbuf, gbuf,
-    lsem, ssem, rsem,
+    qs, ngs, scores, weights, osum, otop, otot, pbuf, sbuf, gbuf,
+    lengths, bias, lsem, ssem, rsem,
 ):
     kv = lax.axis_index("kv")
     tp = lax.axis_index("tp")
     x = lax.rem(kv, X)
     z = kv // X
 
+    def kv_peer(o):
+        a = lax.rem(z + o[0], Z) * X + lax.rem(x + o[1], X)
+        return a, (a, tp)
+
+    def x_peer(o):
+        a = z * X + lax.rem(x + o, X)
+        return a, (a, tp)
+
+    def z_peer(o):
+        a = lax.rem(kv + X * o, KV)
+        return a, (a, tp)
+
+    def tp_peer(o):
+        a = lax.rem(tp // 2 + o[0], TP // 2) * 2 + lax.rem(tp + o[1], 2)
+        return a, (kv, a)
+
+    bar = pltpu.get_barrier_semaphore()
+    greeted = [(tp_peer, o) for o in TP_FAR] + [(z_peer, o) for o in Z_FAR]
+    greeted += [(x_peer, o) for o in X_FAR]
+    for peer, o in greeted:
+        pl.semaphore_signal(bar, inc=1, device_id=peer(o)[1], device_id_type=MESH)
+
     loads = []
 
     def load(src, dst):
@@ -69,6 +106,8 @@
     l_tok = load(tok, tokv)
     l_g1 = load(g1, gainv.at[0])
     l_g2 = load(g2, gainv.at[1])
+    l_len = load(lengths_hbm, lengths)
+    l_bias = load(bias_hbm, bias)
     l_wq = load(wq_hbm, wq)
     l_wk = load(wk_hbm, wkv.at[pl.ds(0, DH)])
     l_wv = load(wv_hbm, wkv.at[pl.ds(DH, DH)])
@@ -80,57 +119,24 @@
     l_wo = load(wo_hbm, wo)
     l_wd = load(wd_hbm, wd.at[pl.ds(0, UNITS)])
 
-    def kv_peer(i):
-        a = lax.rem(kv + i, KV)
-        return a, (a, tp)
-
-    def x_peer(i):
-        a = z * X + lax.rem(x + i, X)
-        return a, (a, tp)
-
-    def z_peer(i):
-        a = lax.rem(kv + X * i, KV)
-        return a, (a, tp)
-
-    def tp_peer(i):
-        a = lax.rem(tp + i, TP)
-        return a, (kv, a)
-
-    bar = pltpu.get_barrier_semaphore()
-
-    def signal_kv(i, c):
-        pl.semaphore_signal(bar, inc=1, device_id=kv_peer(i)[1], device_id_type=MESH)
-        return c
-
-    def signal_tp(i, c):
-        pl.semaphore_signal(bar, inc=1, device_id=tp_peer(i)[1], device_id_type=MESH)
-        return c
-
-    lax.fori_loop(1, KV, signal_kv, 0)
-    lax.fori_loop(1, TP, signal_tp, 0)
-
     waits = []
     used = [0]
 
-    def exchange(n, peer, src_of, buf, slot):
+    def exchange(far, peer, src_of, buf, slot):
         k = used[0]
         used[0] += 1
-
-        def send(i, c):
-            a, dev = peer(i)
+        for o in far:
+            a, dev = peer(o)
             pltpu.make_async_remote_copy(
                 src_ref=src_of(a), dst_ref=buf.at[slot], send_sem=ssem.at[k],
                 recv_sem=rsem.at[k], device_id=dev, device_id_type=MESH,
             ).start()
-            return c
-
-        lax.fori_loop(1, n, send, 0, unroll=True)
-        some = buf.at[pl.ds(0, n - 1)]
+        some = buf.at[pl.ds(0, len(far))]
         waits.append(pltpu.make_async_copy(some, some, ssem.at[k]))
         return pltpu.make_async_copy(some, some, rsem.at[k])
 
-    def spread(n, peer, buf, slot):
-        return exchange(n, peer, lambda a: buf.at[slot], buf, slot)
+    def spread(far, peer, buf, slot):
+        return exchange(far, peer, lambda a: buf.at[slot], buf, slot)
 
     wd[pl.ds(UNITS, WIDE - UNITS), :] = jnp.zeros((WIDE - UNITS, 128), BF16)
     pbuf[...] = jnp.zeros_like(pbuf)
@@ -147,8 +153,8 @@
     c2 = jnp.sum(jnp.where(diag8, gainv[1], 0.0), axis=1, keepdims=True)
     b1[tp] = jnp.where(lane8 == 16, c1, jnp.where(lane8 == 17, c2, 0.0))
     b1[tp, :, 0:B] = tokv[...].astype(F32)
-    pl.semaphore_wait(bar, KV - 1 + TP - 1)
-    r1 = spread(TP, tp_peer, b1, tp)
+    pl.semaphore_wait(bar, len(greeted))
+    r1 = spread(TP_FAR, tp_peer, b1, tp)
     l_wq.wait()
     l_wk.wait()
     l_wv.wait()
@@ -160,6 +166,7 @@
     gain2 = turned[B + 1 : B + 2, :]
     rows16 = rows.astype(BF16)
 
+    scale = DH ** (-0.5)
     lane = iota((B, 128), 1)
     q_part = jnp.dot(rows16, wq[...], preferred_element_type=F32)
     f_all = nt(rows16, wf[...])
@@ -175,18 +182,18 @@
     qx[x, 0:B] = q_part[:, 0:128].astype(BF16)
     qx[x, B : 2 * B] = q_part[:, 128:256].astype(BF16)
     qx[x, 2 * B : 3 * B] = small_tile(f_part, t_part).astype(BF16)
-    r = spread(X, x_peer, qx, x)
+    r = spread(X_FAR, x_peer, qx, x)
     kx[x] = nt(rows16, wkv[...]).astype(BF16)
-    rk = spread(X, x_peer, kx, x)
+    rk = spread(X_FAR, x_peer, kx, x)
     r.wait()
     summed = jnp.sum(qx[...].astype(F32), axis=0)
     small = summed[2 * B : 3 * B]
     qz[z, 0 : 2 * B] = summed[0 : 2 * B].astype(BF16)
     qz[z, 2 * B : 3 * B] = small_tile(lane_sum(small, 0, 3), lane_sum(small, 3, 6)).astype(BF16)
-    r = spread(Z, z_peer, qz, z)
+    r = spread(Z_FAR, z_peer, qz, z)
     rk.wait()
     kz[z] = jnp.sum(kx[...].astype(F32), axis=0).astype(BF16)
-    rk = spread(Z, z_peer, kz, z)
+    rk = spread(Z_FAR, z_peer, kz, z)
 
     l_wg.wait()
     l_wu.wait()
@@ -206,16 +213,19 @@
     bg[kv] = gm[half]
     l_gs.wait()
     l_kv.wait()
+    l_len.wait()
+    l_bias.wait()
 
     r.wait()
     summed = jnp.sum(qz[...].astype(F32), axis=0)
     q0 = summed[0:B].astype(BF16).astype(F32)
     q1 = summed[B : 2 * B].astype(BF16).astype(F32)
+    q0, q1 = q0 * scale, q1 * scale
     small = summed[2 * B : 3 * B]
     tok_mean = lane_sum(small, 3, 6) * (1.0 / D)
     gate_in = lane_sum(small, 0, 3) + bias[tp]
     new_gate = jnp.minimum(gate_in, 0.0) - jnp.log1p(jnp.exp(-jnp.abs(gate_in)))
-    rg = exchange(KV, kv_peer, lambda a: gm.at[lax.rem(a, 2)], bg, kv)
+    rg = exchange(KV_FAR, kv_peer, lambda a: gm.at[lax.rem(a, 2)], bg, kv)
 
     low = lane < DH
     qs[pl.ds(0, B, stride=4), :] = jnp.where(low, q0, 0.0)
@@ -225,26 +235,30 @@
     gate_tile = jnp.broadcast_to(new_gate, (B, 128))
     for j in range(4):
         ngs[pl.ds(j, B, stride=4), :] = gate_tile
-    scale = DH ** (-0.5)
     first = iota((8, POS), 0) < 4
     first128 = iota((8, 128), 0) < 4
     position = iota((8, POS), 1) + kv * POS
     for p in range(B // 2):
         own = pl.ds(8 * p, 8)
         queries = qs[own, :].astype(BF16)
-        s = jnp.where(first, nt(queries, cache[2 * p]), nt(queries, cache[2 * p + 1])) * scale
+        s = jnp.where(first, nt(queries, cache[2 * p]), nt(queries, cache[2 * p + 1]))
         s = s + jnp.where(first, gs[2 * p], gs[2 * p + 1]) + ngs[own, 0:1]
         live = position < jnp.where(first, lengths[2 * p], lengths[2 * p + 1])
-        top = jnp.max(jnp.where(live, s, EMPTY_SCORE), axis=1, keepdims=True)
-        w = jnp.where(live, jnp.exp(s - top), 0.0)
-        w16 = w.astype(BF16)
+        scores[own, :] = jnp.where(live, s, EMPTY_SCORE)
+    s = scores[...]
+    top = jnp.max(s, axis=1, keepdims=True)
+    w = jnp.where(s > 0.5 * EMPTY_SCORE, jnp.exp(s - top), 0.0)
+    otop[...] = jnp.broadcast_to(top, (64, 128))
+    otot[...] = jnp.broadcast_to(jnp.sum(w, axis=1, keepdims=True), (64, 128))
+    weights[...] = w.astype(BF16)
+    for p in range(B // 2):
+        own = pl.ds(8 * p, 8)
+        w16 = weights[own, :]
         osum[own, :] = jnp.where(
             first128,
             jnp.dot(w16, cache[2 * p], preferred_element_type=F32),
             jnp.dot(w16, cache[2 * p + 1], preferred_element_type=F32),
         )
-        otop[own, :] = jnp.broadcast_to(top, (8, 128))
-        otot[own, :] = jnp.broadcast_to(jnp.sum(w, axis=1, keepdims=True), (8, 128))
 
     def by_head(ref):
         return [ref[pl.ds(j, B, stride=4), :] for j in range(4)]
@@ -295,7 +309,7 @@
         return new_sums, new_tops, new_tots
 
     pack(ax, x)
-    r = spread(X, x_peer, ax, x)
+    r = spread(X_FAR, x_peer, ax, x)
     rk.wait()
     keyval = jnp.sum(kz[...].astype(F32), axis=0).astype(BF16).astype(F32)
     turned_kv = pltpu.roll(keyval, DH, 1)
@@ -304,11 +318,11 @@
     owns = []
     for q in (q0, q1):
         prod = q * keys
-        owns.append(jnp.where(low, lane_sum(prod, 0, DH), lane_sum(prod, DH, 128)) * scale)
+        owns.append(jnp.where(low, lane_sum(prod, 0, DH), lane_sum(prod, DH, 128)))
     r.wait()
     sums, tops, tots = unpack(ax, X)
     pack(az, z)
-    r = spread(Z, z_peer, az, z)
+    r = spread(Z_FAR, z_peer, az, z)
     rg.wait()
     gained = jnp.sum(bg[...], axis=0)
     l_wo.wait()
@@ -325,7 +339,7 @@
     proj = jnp.dot(attended[0], wo[0:128, :], preferred_element_type=F32)
     proj = proj + jnp.dot(attended[1], wo[128:256, :], preferred_element_type=F32)
     b4[tp] = proj.astype(BF16)
-    r = spread(TP, tp_peer, b4, tp)
+    r = spread(TP_FAR, tp_peer, b4, tp)
     r.wait()
     centred = rows + jnp.sum(b4[...].astype(F32), axis=0) - tok_mean
 
@@ -343,7 +357,7 @@
                 sbuf[pl.ds(h * 8 + which * 3 + t, B, stride=16), :] = pbuf[which, :, at : at + 128]
     m5[...] = sbuf[...].reshape(KV, 8, 128).astype(BF16)
     b5[kv] = m5[kv]
-    r = exchange(KV, kv_peer, lambda a: m5.at[a], b5, kv)
+    r = exchange(KV_FAR, kv_peer, lambda a: m5.at[a], b5, kv)
     r.wait()
     units = jnp.sum(b5[...].astype(F32), axis=0)
     lane_row = iota((1, 128), 1)
@@ -356,7 +370,7 @@
     hidden = gates / (1.0 + jnp.exp(-gates)) * units[3:6, :]
     b6[kv, 0:3, :] = hidden
     b6[kv, 3:4, :] = jnp.where(lane_row == 0, mean, jnp.where(lane_row == 1, rstd, 0.0))
-    r = spread(KV, kv_peer, b6, kv)
+    r = spread(KV_FAR, kv_peer, b6, kv)
     l_wd.wait()
     r.wait()
     flat = b6.reshape(KV * 4, 128)
@@ -367,7 +381,7 @@
     down = jnp.dot(jnp.concatenate(tiles, axis=1), wd[...], preferred_element_type=F32)
 
     b7[tp] = down.astype(BF16)
-    r = spread(TP, tp_peer, b7, tp)
+    r = spread(TP_FAR, tp_peer, b7, tp)
     mid = (centred - lane_sum(norms, 0, 1)) * lane_sum(norms, 1, 2) * gain1
     mid = mid.astype(BF16).astype(F32)
     r.wait()
@@ -378,7 +392,7 @@
     square2 = jnp.sum(off * off, axis=1, keepdims=True)
     stat = jnp.where(lane == row16, sum2, jnp.where(lane == row16 + B, square2, 0.0))
     b8[kv] = jnp.sum(stat, axis=0, keepdims=True)
-    r = spread(KV, kv_peer, b8, kv)
+    r = spread(KV_FAR, kv_peer, b8, kv)
     r.wait()
     stats = b8[...].reshape(KV, 128)
     total2 = jnp.sum(stats, axis=0, keepdims=True)
@@ -400,13 +414,12 @@
     tokens, live_lengths, kv_cache, gate_sums, w_query, w_key, w_value, w_forget, forget_bias,
     w_out, first_gain, w_gate, w_up, w_down, second_gain,
 ):
-    smem = pl.BlockSpec(memory_space=pltpu.SMEM)
     hbm = pl.BlockSpec(memory_space=pl.ANY)
     vmem = pltpu.VMEM
     turned = pl.pallas_call(
         kernel,
         out_shape=jax.ShapeDtypeStruct((8, B), BF16),
-        in_specs=[smem, smem] + [hbm] * 13,
+        in_specs=[hbm] * 15,
         out_specs=pl.BlockSpec(memory_space=pltpu.VMEM),
         scratch_shapes=[
             vmem((B, POS, 128), BF16),
@@ -437,13 +450,17 @@
             vmem((KV, 1, 128), F32),
             vmem((64, 128), F32),
             vmem((64, 128), F32),
+            vmem((64, POS), F32),
+            vmem((64, POS), BF16),
             vmem((64, 128), F32),
             vmem((64, 128), F32),
             vmem((64, 128), F32),
             vmem((2, B, WIDE), F32),
             vmem((KV * 8, 128), F32),
             vmem((2, WIDE), F32),
-            pltpu.SemaphoreType.DMA((13,)),
+            pltpu.SMEM((B,), jnp.int32),
+            pltpu.SMEM((TP,), F32),
+            pltpu.SemaphoreType.DMA((15,)),
             pltpu.SemaphoreType.DMA((13,)),
             pltpu.SemaphoreType.DMA((13,)),
         ],

time: 73.8 us -> 68.3 us (0.925)
  Pallas kernels: 72.4 us -> 66.9 us
    pallas_call x1, Pallas kernels: 72.4 us -> 66.9 us  [on_device(): pl.pallas_call(kernel, out_shape=jax.ShapeDtypeStruct((8, B), BF16), in_s...]
where the time goes in v2:
time: 68.3 us; the launch traced here: 68.2 us
  Pallas kernels  66.9 us (98%)
  local copies, waits for them, and re-layouts  1.26 us (2%)
    pallas_call x1, Pallas kernels, on_device(): pl.pallas_call(kernel, out_shape=jax.ShapeDtypeStruct((8, B), BF16), in_s...  66.9 us

profile of v2, /device:TPU:1, one launch (start us, length us, event | category | flops | bytes accessed | tf_op | source)
XLA Modules:
  0.0 68.2 jit_solution(16078899135611511756)
XLA Ops:
  0.0 66.9 %shard_map.145 = bf16[8,16]{1,0:T(8,128)(2,1)} custom-call(s32[16]{0:T(128)} %lengths_hbm.1, f32[16]{0:T(128)} %bias_hbm.1, bf16[8,16]{1,0:T(8,128)(2,1)} %bitcast.15, f32[1,8]{1,0:T(1,128)} %bitcast.16, f32[1,8]{1,0:T(1,128)} %bitcast.17, bf16[16,512,128]{2,1,0:T(8,128)(2,1)} %kv_hbm.1, f32[16,1,512]{2,1,0:T(1,128)} %gs_hbm.1, bf16[128,256]{1,0:T(8,128)(2,1)} %wq_hbm.1, ...), custom_call_target="tpu_custom_call" | custom-call | tf_op jit(solution)/shard_map/pallas_call | solution.py:419
  66.9 1.3 %copy.17 = bf16[16,8]{0,1:T(8,128)(2,1)} copy(bf16[16,8]{0,1:T(8,128)(2,1)} %bitcast.14) | data formatting | bytes 512

commit v3 on v2

--- a/solution.py
+++ b/solution.py
@@ -64,9 +64,9 @@
     wu_hbm, wd_hbm, out,
     cache, gs, wq, wkv, wf, wo, wg, wu, wd,
     tokv, gainv,
-    b1, qx, qz, kx, kz, ax, az, b4, gm, bg, m5, b5, b6, b7, b8,
-    qs, ngs, scores, weights, osum, otop, otot, pbuf, sbuf, gbuf,
-    lengths, bias, lsem, ssem, rsem,
+    b1, qa, qb, pairs, m2, b2, aa, ab, sa, sb, b4, gm, bg, m5, b5, b6, b7, b8,
+    qs, ngs, scores, weights, osum, otop, otot, pbuf, sbuf, gbuf, gtile,
+    lengths, bias, plane, lsem, ssem, rsem,
 ):
     kv = lax.axis_index("kv")
     tp = lax.axis_index("tp")
@@ -122,18 +122,25 @@
     waits = []
     used = [0]
 
-    def exchange(far, peer, src_of, buf, slot):
+    def both(far, peer, pieces, slot):
         k = used[0]
-        used[0] += 1
+        used[0] += len(pieces)
         for o in far:
             a, dev = peer(o)
-            pltpu.make_async_remote_copy(
-                src_ref=src_of(a), dst_ref=buf.at[slot], send_sem=ssem.at[k],
-                recv_sem=rsem.at[k], device_id=dev, device_id_type=MESH,
-            ).start()
-        some = buf.at[pl.ds(0, len(far))]
-        waits.append(pltpu.make_async_copy(some, some, ssem.at[k]))
-        return pltpu.make_async_copy(some, some, rsem.at[k])
+            for n, (src_of, buf) in enumerate(pieces):
+                pltpu.make_async_remote_copy(
+                    src_ref=src_of(a), dst_ref=buf.at[slot], send_sem=ssem.at[k + n],
+                    recv_sem=rsem.at[k + n], device_id=dev, device_id_type=MESH,
+                ).start()
+        got = []
+        for n, (_, buf) in enumerate(pieces):
+            some = buf.at[pl.ds(0, len(far))]
+            waits.append(pltpu.make_async_copy(some, some, ssem.at[k + n]))
+            got.append(pltpu.make_async_copy(some, some, rsem.at[k + n]))
+        return got
+
+    def exchange(far, peer, src_of, buf, slot):
+        return both(far, peer, ((src_of, buf),), slot)[0]
 
     def spread(far, peer, buf, slot):
         return exchange(far, peer, lambda a: buf.at[slot], buf, slot)
@@ -142,7 +149,7 @@
     pbuf[...] = jnp.zeros_like(pbuf)
     gbuf[...] = jnp.zeros_like(gbuf)
     sbuf[...] = jnp.zeros_like(sbuf)
-    gm[...] = jnp.zeros_like(gm)
+    gtile[...] = jnp.zeros_like(gtile)
 
     l_tok.wait()
     l_g1.wait()
@@ -154,6 +161,8 @@
     b1[tp] = jnp.where(lane8 == 16, c1, jnp.where(lane8 == 17, c2, 0.0))
     b1[tp, :, 0:B] = tokv[...].astype(F32)
     pl.semaphore_wait(bar, len(greeted))
+    for o in X_FAR:
+        pl.semaphore_signal(plane, inc=1, device_id=x_peer(o)[1], device_id_type=MESH)
     r1 = spread(TP_FAR, tp_peer, b1, tp)
     l_wq.wait()
     l_wk.wait()
@@ -179,21 +188,22 @@
             tile = jnp.where(lane == k, piece, tile)
         return tile
 
-    qx[x, 0:B] = q_part[:, 0:128].astype(BF16)
-    qx[x, B : 2 * B] = q_part[:, 128:256].astype(BF16)
-    qx[x, 2 * B : 3 * B] = small_tile(f_part, t_part).astype(BF16)
-    r = spread(X_FAR, x_peer, qx, x)
-    kx[x] = nt(rows16, wkv[...]).astype(BF16)
-    rk = spread(X_FAR, x_peer, kx, x)
-    r.wait()
-    summed = jnp.sum(qx[...].astype(F32), axis=0)
-    small = summed[2 * B : 3 * B]
-    qz[z, 0 : 2 * B] = summed[0 : 2 * B].astype(BF16)
-    qz[z, 2 * B : 3 * B] = small_tile(lane_sum(small, 0, 3), lane_sum(small, 3, 6)).astype(BF16)
-    r = spread(Z_FAR, z_peer, qz, z)
-    rk.wait()
-    kz[z] = jnp.sum(kx[...].astype(F32), axis=0).astype(BF16)
-    rk = spread(Z_FAR, z_peer, kz, z)
+    for half, buf in enumerate((qa, qb)):
+        few = slice(8 * half, 8 * half + 8)
+        buf[kv] = jnp.concatenate([q_part[few, 0:128], q_part[few, 128:256]], axis=0).astype(BF16)
+    pl.semaphore_wait(plane, len(X_FAR))
+    new_pairs = nt(rows16, wkv[...])
+    flat = pairs.reshape(KV * 2, 128)
+    gates = jnp.zeros((B, 128), F32)
+    for k, piece in enumerate(split3(f_part)):
+        gates = jnp.where(lane == k, piece, gates)
+    for h in range(2):
+        flat[pl.ds(2 * h, B, stride=4), :] = new_pairs
+        flat[pl.ds(2 * h + 1, B, stride=4), :] = gates
+    m2[...] = pairs[...].astype(BF16)
+    b2[kv] = m2[kv]
+    rk, ra = both(KV_FAR, kv_peer, ((lambda a: m2.at[a], b2), (lambda a: qa.at[kv], qa)), kv)
+    rb = spread(KV_FAR, kv_peer, qb, kv)
 
     l_wg.wait()
     l_wu.wait()
@@ -207,139 +217,120 @@
     for h in range(2):
         for t in range(3):
             at = (h * 3 + t) * 128
-            gm[h, t : t + 1, :] = gbuf[0:1, at : at + 128]
-            gm[h, 3 + t : 4 + t, :] = gbuf[1:2, at : at + 128]
-    half = lax.rem(kv, 2)
-    bg[kv] = gm[half]
+            gtile[h, t : t + 1, :] = gbuf[0:1, at : at + 128]
+            gtile[h, 3 + t : 4 + t, :] = gbuf[1:2, at : at + 128]
+    gm[...] = gtile[...].astype(BF16)
+    bg[kv] = gm[lax.rem(kv, 2)]
     l_gs.wait()
     l_kv.wait()
     l_len.wait()
     l_bias.wait()
 
-    r.wait()
-    summed = jnp.sum(qz[...].astype(F32), axis=0)
-    q0 = summed[0:B].astype(BF16).astype(F32)
-    q1 = summed[B : 2 * B].astype(BF16).astype(F32)
-    q0, q1 = q0 * scale, q1 * scale
-    small = summed[2 * B : 3 * B]
-    tok_mean = lane_sum(small, 3, 6) * (1.0 / D)
-    gate_in = lane_sum(small, 0, 3) + bias[tp]
-    new_gate = jnp.minimum(gate_in, 0.0) - jnp.log1p(jnp.exp(-jnp.abs(gate_in)))
-    rg = exchange(KV_FAR, kv_peer, lambda a: gm.at[lax.rem(a, 2)], bg, kv)
-
-    low = lane < DH
-    qs[pl.ds(0, B, stride=4), :] = jnp.where(low, q0, 0.0)
-    qs[pl.ds(1, B, stride=4), :] = jnp.where(low, pltpu.roll(q0, DH, 1), 0.0)
-    qs[pl.ds(2, B, stride=4), :] = jnp.where(low, q1, 0.0)
-    qs[pl.ds(3, B, stride=4), :] = jnp.where(low, pltpu.roll(q1, DH, 1), 0.0)
-    gate_tile = jnp.broadcast_to(new_gate, (B, 128))
-    for j in range(4):
-        ngs[pl.ds(j, B, stride=4), :] = gate_tile
     first = iota((8, POS), 0) < 4
     first128 = iota((8, 128), 0) < 4
     position = iota((8, POS), 1) + kv * POS
-    for p in range(B // 2):
-        own = pl.ds(8 * p, 8)
-        queries = qs[own, :].astype(BF16)
-        s = jnp.where(first, nt(queries, cache[2 * p]), nt(queries, cache[2 * p + 1]))
-        s = s + jnp.where(first, gs[2 * p], gs[2 * p + 1]) + ngs[own, 0:1]
-        live = position < jnp.where(first, lengths[2 * p], lengths[2 * p + 1])
-        scores[own, :] = jnp.where(live, s, EMPTY_SCORE)
-    s = scores[...]
-    top = jnp.max(s, axis=1, keepdims=True)
-    w = jnp.where(s > 0.5 * EMPTY_SCORE, jnp.exp(s - top), 0.0)
-    otop[...] = jnp.broadcast_to(top, (64, 128))
-    otot[...] = jnp.broadcast_to(jnp.sum(w, axis=1, keepdims=True), (64, 128))
-    weights[...] = w.astype(BF16)
-    for p in range(B // 2):
-        own = pl.ds(8 * p, 8)
-        w16 = weights[own, :]
-        osum[own, :] = jnp.where(
-            first128,
-            jnp.dot(w16, cache[2 * p], preferred_element_type=F32),
-            jnp.dot(w16, cache[2 * p + 1], preferred_element_type=F32),
-        )
-
-    def by_head(ref):
-        return [ref[pl.ds(j, B, stride=4), :] for j in range(4)]
-
-    os, tops, tots = by_head(osum), by_head(otop), by_head(otot)
-    sums = [jnp.where(low, pltpu.roll(os[2 * i], DH, 1), os[2 * i + 1]) for i in range(2)]
-    tops = [jnp.where(low, tops[2 * i], tops[2 * i + 1]) for i in range(2)]
-    tots = [jnp.where(low, tots[2 * i], tots[2 * i + 1]) for i in range(2)]
-
-    place = lax.rem(lane, DH)
-
-    def pack(buf, slot):
-        buf[slot, 0:B] = sums[0].astype(BF16)
-        buf[slot, B : 2 * B] = sums[1].astype(BF16)
-        tile = jnp.zeros((B, 128), F32)
-        k = 0
-        for v in (*tops, *tots):
-            for piece in split3(v):
-                tile = jnp.where(place == k, piece, tile)
-                k += 1
-        buf[slot, 2 * B : 3 * B] = tile.astype(BF16)
-
-    src = iota((128, 512), 0)
-    dst = iota((128, 512), 1)
-    wanted = 3 * (dst // 128)
-    pick = (src // DH == lax.rem(dst, 128) // DH) & (lax.rem(src, DH) >= wanted)
-    pick = jnp.where(pick & (lax.rem(src, DH) < wanted + 3), 1.0, 0.0).astype(BF16)
-
-    def unpack(buf, n):
-        spreads = [
-            jnp.dot(buf[i, 2 * B : 3 * B], pick, preferred_element_type=F32) for i in range(n)
-        ]
-        new_sums, new_tops, new_tots = [], [], []
-        for c in range(2):
-            t = [v[:, c * 128 : c * 128 + 128] for v in spreads]
-            u = [v[:, 256 + c * 128 : 384 + c * 128] for v in spreads]
-            top = t[0]
-            for v in t[1:]:
-                top = jnp.maximum(top, v)
-            total, weighted = 0.0, 0.0
-            for i in range(n):
-                e = jnp.exp(t[i] - top)
-                total = total + u[i] * e
-                weighted = weighted + buf[i, c * B : c * B + B].astype(F32) * e
-            new_sums.append(weighted)
-            new_tops.append(top)
-            new_tots.append(total)
-        return new_sums, new_tops, new_tots
-
-    pack(ax, x)
-    r = spread(X_FAR, x_peer, ax, x)
-    rk.wait()
-    keyval = jnp.sum(kz[...].astype(F32), axis=0).astype(BF16).astype(F32)
-    turned_kv = pltpu.roll(keyval, DH, 1)
-    keys = jnp.where(low, keyval, turned_kv)
-    values = jnp.where(low, turned_kv, keyval)
-    owns = []
-    for q in (q0, q1):
-        prod = q * keys
-        owns.append(jnp.where(low, lane_sum(prod, 0, DH), lane_sum(prod, DH, 128)))
-    r.wait()
-    sums, tops, tots = unpack(ax, X)
-    pack(az, z)
-    r = spread(Z_FAR, z_peer, az, z)
-    rg.wait()
-    gained = jnp.sum(bg[...], axis=0)
+    low8 = iota((8, 128), 1) < DH
+    row32 = iota((32, 128), 0)
+    lane32 = iota((32, 128), 1)
+
+    own_pair = []
+
+    def attend(half, buf):
+        base = 32 * half
+        rows32 = pl.ds(base, 32)
+        summed = jnp.sum(buf[...].astype(F32), axis=0).astype(BF16).astype(F32) * scale
+        tiles = (summed[0:8], summed[8:16])
+        for j in range(4):
+            t = tiles[j // 2]
+            t = pltpu.roll(t, DH, 1) if j % 2 else t
+            qs[pl.ds(base + j, 8, stride=4), :] = jnp.where(low8, t, 0.0)
+        for p in range(4 * half, 4 * half + 4):
+            own = pl.ds(8 * p, 8)
+            queries = qs[own, :].astype(BF16)
+            s = jnp.where(first, nt(queries, cache[2 * p]), nt(queries, cache[2 * p + 1]))
+            s = s + jnp.where(first, gs[2 * p], gs[2 * p + 1])
+            live = position < jnp.where(first, lengths[2 * p], lengths[2 * p + 1])
+            scores[own, :] = jnp.where(live, s, EMPTY_SCORE)
+        if not own_pair:
+            rk.wait()
+            own_pair.append(jnp.sum(b2[...].astype(F32), axis=0))
+        pair = own_pair[0][0:1, :].astype(BF16).astype(F32)
+        own_value = pair
+        gate_in = lane_sum(own_pair[0][1:2, :], 0, 3) + bias[tp]
+        new_gate = jnp.minimum(gate_in, 0.0) - jnp.log1p(jnp.exp(-jnp.abs(gate_in)))
+        own_score = jnp.sum(qs[rows32, :] * pair, axis=1, keepdims=True) - new_gate
+        here = (row32[:, 0:1] // 2) == kv - 16 * half
+        own_score = jnp.where(here, own_score, EMPTY_SCORE)
+        s = scores[rows32, :]
+        top = jnp.maximum(jnp.max(s, axis=1, keepdims=True), own_score)
+        own_weight = jnp.where(here, jnp.exp(own_score - top), 0.0)
+        w = jnp.where(s > 0.5 * EMPTY_SCORE, jnp.exp(s - top), 0.0)
+        total = jnp.sum(w, axis=1, keepdims=True) + own_weight
+        weights[rows32, :] = w.astype(BF16)
+        for p in range(4 * half, 4 * half + 4):
+            own = pl.ds(8 * p, 8)
+            w16 = weights[own, :]
+            osum[own, :] = jnp.where(
+                first128,
+                jnp.dot(w16, cache[2 * p], preferred_element_type=F32),
+                jnp.dot(w16, cache[2 * p + 1], preferred_element_type=F32),
+            )
+        osum[rows32, :] = osum[rows32, :] + own_weight.astype(BF16).astype(F32) * own_value
+        o = [osum[pl.ds(base + j, 8, stride=4), :] for j in range(4)]
+        sums = [jnp.where(low8, pltpu.roll(o[2 * i], DH, 1), o[2 * i + 1]) for i in range(2)]
+        stat = jnp.where(lane32 == row32, top, jnp.where(lane32 == row32 + 32, total, 0.0))
+        return jnp.concatenate(sums, axis=0), jnp.sum(stat, axis=0, keepdims=True)
+
+    mask8 = lax.rem(iota((8, 128), 1), 32) // 4 == iota((8, 128), 0)
+    source = iota((128, 256), 0)
+    pick = lax.rem(source, 4) == iota((128, 256), 1) // DH
+    pick = jnp.where(pick & (source < 96), 1.0, 0.0).astype(BF16)
+
+    def combine(buf, stats):
+        stat = stats[...].reshape(KV, 128)
+        joint = jnp.max(stat, axis=0, keepdims=True)
+        e = jnp.exp(stat - joint)
+        total = jnp.sum(pltpu.roll(stat, 96, 1) * e, axis=0, keepdims=True)
+        factors = jnp.concatenate([e, total], axis=0)
+        hi, mid, low_part = split3(jnp.where(iota(factors.shape, 1) < 32, factors, 0.0))
+        packed = hi + pltpu.roll(mid, 32, 1) + pltpu.roll(low_part, 64, 1)
+        wide = [jnp.where(mask8, packed[i : i + 1, :], 0.0) for i in range(KV + 1)]
+        wide = jnp.concatenate(wide, axis=0).astype(BF16)
+        wide = jnp.dot(wide, pick, preferred_element_type=F32)
+        acc = [0.0, 0.0]
+        for i in range(KV):
+            part = buf[i].astype(F32)
+            for c in range(2):
+                acc[c] = acc[c] + part[8 * c : 8 * c + 8] * wide[8 * i : 8 * i + 8, 128 * c : 128 * c + 128]
+        return [acc[c] / wide[8 * KV :, 128 * c : 128 * c + 128] for c in range(2)]
+
+    ra.wait()
+    message, stat = attend(0, qa)
+    aa[kv] = message.astype(BF16)
+    tok_row = jnp.sum(jnp.where(lane == row16 + 64, t_part, 0.0), axis=0, keepdims=True)
+    sa[kv] = stat + tok_row
+    got_a = both(KV_FAR, kv_peer, ((lambda a: sa.at[kv], sa), (lambda a: aa.at[kv], aa)), kv)
+    rb.wait()
+    message, stat = attend(1, qb)
+    ab[kv] = message.astype(BF16)
+    sb[kv] = stat
+    got_b = both(KV_FAR, kv_peer, ((lambda a: sb.at[kv], sb), (lambda a: ab.at[kv], ab)), kv)
     l_wo.wait()
-    r.wait()
-    sums, tops, tots = unpack(az, Z)
-    attended = []
-    for c in range(2):
-        final = jnp.maximum(tops[c], owns[c])
-        carry = jnp.exp(tops[c] - final)
-        own_weight = jnp.exp(owns[c] - final)
-        top_part = sums[c] * carry + own_weight.astype(BF16).astype(F32) * values
-        attended.append((top_part / (tots[c] * carry + own_weight)).astype(BF16))
+    for r in got_a:
+        r.wait()
+    part_a = combine(aa, sa)
+    tok_total = jnp.sum(sa[...].reshape(KV, 128), axis=0, keepdims=True)
+    tok_mean = jnp.sum(jnp.where(lane == row16 + 64, tok_total, 0.0), axis=1, keepdims=True) * (1.0 / D)
+    for r in got_b:
+        r.wait()
+    part_b = combine(ab, sb)
+    attended = [jnp.concatenate([part_a[c], part_b[c]], axis=0).astype(BF16) for c in range(2)]
 
     proj = jnp.dot(attended[0], wo[0:128, :], preferred_element_type=F32)
     proj = proj + jnp.dot(attended[1], wo[128:256, :], preferred_element_type=F32)
     b4[tp] = proj.astype(BF16)
     r = spread(TP_FAR, tp_peer, b4, tp)
+    rg = exchange(KV_FAR, kv_peer, lambda a: gm.at[lax.rem(a, 2)], bg, kv)
     r.wait()
     centred = rows + jnp.sum(b4[...].astype(F32), axis=0) - tok_mean
 
@@ -358,6 +349,8 @@
     m5[...] = sbuf[...].reshape(KV, 8, 128).astype(BF16)
     b5[kv] = m5[kv]
     r = exchange(KV_FAR, kv_peer, lambda a: m5.at[a], b5, kv)
+    rg.wait()
+    gained = jnp.sum(bg[...].astype(F32), axis=0)
     r.wait()
     units = jnp.sum(b5[...].astype(F32), axis=0)
     lane_row = iota((1, 128), 1)
@@ -418,7 +411,7 @@
     vmem = pltpu.VMEM
     turned = pl.pallas_call(
         kernel,
-        out_shape=jax.ShapeDtypeStruct((8, B), BF16),
+        out_shape=pltpu.VMEM((8, B), BF16),
         in_specs=[hbm] * 15,
         out_specs=pl.BlockSpec(memory_space=pltpu.VMEM),
         scratch_shapes=[
@@ -434,15 +427,18 @@
             vmem((8, B), BF16),
             vmem((2, 1, 8), F32),
             vmem((TP, 8, 128), F32),
-            vmem((X, 3 * B, 128), BF16),
-            vmem((Z, 3 * B, 128), BF16),
-            vmem((X, B, 128), BF16),
-            vmem((Z, B, 128), BF16),
-            vmem((X, 3 * B, 128), BF16),
-            vmem((Z, 3 * B, 128), BF16),
+            vmem((KV, B, 128), BF16),
+            vmem((KV, B, 128), BF16),
+            vmem((KV, 2, 128), F32),
+            vmem((KV, 2, 128), BF16),
+            vmem((KV, 2, 128), BF16),
+            vmem((KV, B, 128), BF16),
+            vmem((KV, B, 128), BF16),
+            vmem((KV, 1, 128), F32),
+            vmem((KV, 1, 128), F32),
             vmem((TP, B, 128), BF16),
-            vmem((2, 8, 128), F32),
-            vmem((KV, 8, 128), F32),
+            vmem((2, 8, 128), BF16),
+            vmem((KV, 8, 128), BF16),
             vmem((KV, 8, 128), BF16),
             vmem((KV, 8, 128), BF16),
             vmem((KV, 4, 128), F32),
@@ -458,11 +454,13 @@
             vmem((2, B, WIDE), F32),
             vmem((KV * 8, 128), F32),
             vmem((2, WIDE), F32),
+            vmem((2, 8, 128), F32),
             pltpu.SMEM((B,), jnp.int32),
             pltpu.SMEM((TP,), F32),
+            pltpu.SemaphoreType.REGULAR,
             pltpu.SemaphoreType.DMA((15,)),
-            pltpu.SemaphoreType.DMA((13,)),
-            pltpu.SemaphoreType.DMA((13,)),
+            pltpu.SemaphoreType.DMA((14,)),
+            pltpu.SemaphoreType.DMA((14,)),
         ],
         compiler_params=pltpu.CompilerParams(collective_id=0, has_side_effects=True),
     )(

time: 68.3 us -> 65.5 us (0.959)
  Pallas kernels: 66.9 us -> 64.8 us
    pallas_call x1, Pallas kernels: 66.9 us -> 64.8 us  [on_device(): pl.pallas_call(kernel, out_shape=pltpu.VMEM((8, B), BF16), in_specs=[hbm]...]
where the time goes in v3:
time: 65.5 us; the launch traced here: 65.4 us
  Pallas kernels  64.8 us (99%)
    pallas_call x1, Pallas kernels, on_device(): pl.pallas_call(kernel, out_shape=pltpu.VMEM((8, B), BF16), in_specs=[hbm]...  64.8 us

profile of v3, /device:TPU:1, one launch (start us, length us, event | category | flops | bytes accessed | tf_op | source)
XLA Modules:
  0.0 65.4 jit_solution(9558046664295803602)
XLA Ops:
  0.0 64.8 %shard_map.145 = bf16[8,16]{1,0:T(8,128)(2,1)S(1)} custom-call(s32[16]{0:T(128)} %lengths_hbm.1, f32[16]{0:T(128)} %bias_hbm.1, bf16[8,16]{1,0:T(8,128)(2,1)} %bitcast.15, f32[1,8]{1,0:T(1,128)} %bitcast.16, f32[1,8]{1,0:T(1,128)} %bitcast.17, bf16[16,512,128]{2,1,0:T(8,128)(2,1)} %kv_hbm.1, f32[16,1,512]{2,1,0:T(1,128)} %gs_hbm.1, bf16[128,256]{1,0:T(8,128)(2,1)} %wq_hbm.1, ...), custom_call_target="tpu_custom_call" | custom-call | tf_op jit(solution)/shard_map/pallas_call | solution.py:412
  64.8 0.6 copy.17
